TPU v7x, 32 devices: a whole 2x2x4 slice. The times are simulated.
32 devices in a mesh: grp: 2 (over y), ep: 4 (over z), tp: 4 (over x, core).
Axes of the slice: x: 2, y: 2, z: 4, core: 2. Of those that a mesh axis runs over, the one named last changes fastest.
Arguments:
- queries: bfloat16 [16384, 1024], P(('grp', 'ep'), 'tp'), parts along dimension 0, may hold values from -6 to 6
- key_vectors: bfloat16 [16384, 1024], P(('grp', 'ep'), 'tp'), parts along dimension 0, may hold values from -6 to 6
- value_vectors: bfloat16 [16384, 1024], P(('grp', 'ep'), 'tp'), parts along dimension 0, may hold values from -6 to 6
- input_gate: float32 [16384, 16], P(('grp', 'ep'), 'tp'), parts along dimension 0, may hold values from -6 to 320
- forget_gate: float32 [16384, 16], P(('grp', 'ep'), 'tp'), parts along dimension 0, may hold values from 0 to 15
- head_gain: float32 [1024], P('tp'), may hold values from 0.1 to 1.9
- out_weight: bfloat16 [1024, 2048], P(None, 'tp'), may hold values from -0.1875 to 0.1875
- expert_input: bfloat16 [1024, 2048], P(('grp', 'ep')), parts along dimension 0, may hold values from -6 to 6
- norm_gain: float32 [2048], replicated, may hold values from 0.1 to 1.9
- routes: int32 [1024, 2], P(('grp', 'ep')), parts along dimension 0, may hold values from 0 to 3, all different within a row; in each aligned block of 128 rows (0 to 127, 128 to 255, ...) at most 80 rows name the same one
- route_weight: float32 [1024, 2], P(('grp', 'ep')), parts along dimension 0, may hold values from 0.25 to 1
- gate_weight: bfloat16 [4, 2048, 3584], P('ep', None, 'tp'), may hold values from -0.125 to 0.125
- up_weight: bfloat16 [4, 2048, 3584], P('ep', None, 'tp'), may hold values from -0.125 to 0.125
- down_weight: bfloat16 [4, 3584, 2048], P('ep', 'tp'), may hold values from -0.125 to 0.125
Outputs:
- mixer_out: bfloat16 [16384, 2048], P(('grp', 'ep'), 'tp'), parts along dimension 0
- expert_out: bfloat16 [1024, 2048], P(('grp', 'ep'), 'tp'), parts along dimension 0
There are 2 independent parts, one for each index of `grp`. A program takes and returns all parts, laid end to end along the dimension named above; an argument that names none is the same for every part. Nothing has to cross between parts.
Inputs may be any that keep to these rules, and one draw needn't show every extreme that they name: `routes`: A token's 2 experts differ. Among the 128 tokens of one index of ep, no expert is named more than 80 times, and in some of these blocks one is named exactly 80 times.
All inputs are finite; a program needn't handle non-finite values.
Results may differ from a plain program's by a relative error of at most 0.019.
Values may be sent and summed in bfloat16 or wider, within the bound.
A program may use at most 64 MiB of HBM per device.

v0:
```python
import jax
import jax.numpy as jnp
from jax import lax
from jax.sharding import PartitionSpec as P

HEAD = 64
BLK = 128


EXACT_PRECISION = lax.Precision.HIGHEST
VERY_NEGATIVE = -1e30


def prefix(part, axis, combine, identity):
    place = lax.axis_index(axis)
    gathered = jax.tree.map(lambda a: lax.all_gather(a, axis), part)
    state = jax.tree.map(lambda a, e: jnp.zeros_like(a) + jnp.asarray(e, a.dtype), part, identity)

    def one(step, state):
        return combine(
            state, jax.tree.map(lambda a: lax.dynamic_index_in_dim(a, step, 0, False), gathered)
        )

    return lax.fori_loop(0, place, one, state)


def combine_states(before_part, after_part):
    decay_early, matrix_early, normer_early, stable_early = before_part
    decay_late, matrix_late, normer_late, stable_late = after_part
    highest = jnp.maximum(decay_late + stable_early, stable_late)
    scale_early = jnp.exp(decay_late + stable_early - highest)
    scale_late = jnp.exp(stable_late - highest)
    matrix_joined = (
        scale_early[..., None, None] * matrix_early + scale_late[..., None, None] * matrix_late
    )
    normer_joined = scale_early[..., None] * normer_early + scale_late[..., None] * normer_late
    return (decay_early + decay_late, matrix_joined, normer_joined, highest)


def memory_cells(queries, key_vectors, value_vectors, input_gate, forget_gate, head_gain):
    segment_len = input_gate.shape[0]
    heads = input_gate.shape[1]
    blocks = segment_len // BLK
    head_scale = HEAD ** (-0.5)

    def block_view(matrix):
        return matrix.reshape(blocks, BLK, heads, HEAD).transpose(2, 0, 1, 3)

    query_blocks = block_view(queries)
    key_blocks = block_view(key_vectors)
    value_blocks = block_view(value_vectors)
    input_blocks = input_gate.reshape(blocks, BLK, heads).transpose(2, 0, 1)
    log_forget = jax.nn.log_sigmoid(forget_gate).reshape(blocks, BLK, heads).transpose(2, 0, 1)
    running_decay = jnp.cumsum(log_forget, axis=-1)
    block_end = running_decay[..., -1]
    tail_gate = block_end[..., None] - running_decay + input_blocks
    block_peak = jnp.max(tail_gate, axis=-1)
    key_weight = jnp.exp(tail_gate - block_peak[..., None])
    key_weighted_rows = (key_weight[..., None] * key_blocks).astype(jnp.bfloat16)
    matrix_terms = jnp.einsum(
        "hcsk,hcsv->hckv", key_weighted_rows, value_blocks, preferred_element_type=jnp.float32
    )
    normer_terms = jnp.sum(key_weighted_rows.astype(jnp.float32), axis=2)
    inclusive = lax.associative_scan(
        combine_states, (block_end, matrix_terms, normer_terms, block_peak), axis=1
    )
    device_total = tuple((member[:, -1] for member in inclusive))
    identity = (
        jnp.zeros((heads,), jnp.float32),
        jnp.zeros((heads, HEAD, HEAD), jnp.float32),
        jnp.zeros((heads, HEAD), jnp.float32),
        jnp.full((heads,), VERY_NEGATIVE, jnp.float32),
    )
    earlier_states = prefix(device_total, "ep", combine_states, identity)
    initial = (
        jnp.zeros((heads,), jnp.float32),
        jnp.zeros((heads, HEAD, HEAD), jnp.float32),
        jnp.zeros((heads, HEAD), jnp.float32),
        jnp.zeros((heads,), jnp.float32),
    )
    entering = combine_states(initial, earlier_states)
    local_entry = tuple(
        (
            jnp.concatenate([start_value[:, None], member[:, :-1]], axis=1)
            for start_value, member in zip(identity, inclusive)
        )
    )
    incoming = tuple((member[:, None] for member in entering))
    ignored, matrix_entry, normer_entry, stable_entry = combine_states(incoming, local_entry)
    causal = jnp.arange(BLK)[:, None] >= jnp.arange(BLK)[None, :]
    log_weights = (
        running_decay[..., :, None] - running_decay[..., None, :] + input_blocks[..., None, :]
    )
    log_weights = jnp.where(causal, log_weights, -jnp.inf)
    stabilizer = jnp.maximum(running_decay + stable_entry[..., None], jnp.max(log_weights, axis=-1))
    scores = (
        jnp.einsum("hcjd,hcsd->hcjs", query_blocks, key_blocks, preferred_element_type=jnp.float32)
        * head_scale
    )
    weighted = jnp.exp(log_weights - stabilizer[..., None]) * scores
    carried_scale = jnp.exp(running_decay + stable_entry[..., None] - stabilizer)
    query_wide = query_blocks.astype(jnp.float32)
    carried = (
        jnp.einsum("hcjk,hckv->hcjv", query_wide, matrix_entry, precision=EXACT_PRECISION)
        * head_scale
    )
    numerator = carried_scale[..., None] * carried + jnp.einsum(
        "hcjs,hcsv->hcjv",
        weighted.astype(jnp.bfloat16),
        value_blocks,
        preferred_element_type=jnp.float32,
    )
    denominator = carried_scale * jnp.einsum(
        "hcjk,hck->hcj", query_wide, normer_entry, precision=EXACT_PRECISION
    ) * head_scale + jnp.sum(weighted, axis=-1)
    cells = numerator / jnp.maximum(jnp.abs(denominator), jnp.exp(-stabilizer))[..., None]
    normed = cells * lax.rsqrt(jnp.mean(cells * cells, axis=-1, keepdims=True) + 1e-06)
    normed = (normed * head_gain.reshape(heads, 1, 1, HEAD)).astype(jnp.bfloat16)
    return normed.transpose(1, 2, 0, 3).reshape(segment_len, heads * HEAD)


def on_device(
    queries,
    key_vectors,
    value_vectors,
    input_gate,
    forget_gate,
    head_gain,
    out_weight,
    expert_input,
    norm_gain,
    routes,
    route_weight,
    gate_weight,
    up_weight,
    down_weight,
):
    normed = memory_cells(queries, key_vectors, value_vectors, input_gate, forget_gate, head_gain)
    mixer_out = jnp.dot(
        lax.all_gather(normed, "tp", axis=1, tiled=True),
        out_weight,
        preferred_element_type=jnp.float32,
    ).astype(jnp.bfloat16)
    tokens = expert_input.shape[0]
    row_width = expert_input.shape[1]
    choices_per = routes.shape[1]
    experts = lax.axis_size("ep")
    splits = lax.axis_size("tp")
    slice_width = row_width // splits
    capacity = 5 * tokens * choices_per // (4 * experts)
    input_wide = expert_input.astype(jnp.float32)
    scaled = input_wide * lax.rsqrt(
        jnp.mean(input_wide * input_wide, axis=-1, keepdims=True) + 1e-06
    )
    scaled = scaled * norm_gain
    chosen = routes.reshape(-1)
    onehot = (chosen[:, None] == jnp.arange(experts, dtype=jnp.int32)[None, :]).astype(jnp.int32)
    slot_index = jnp.sum((jnp.cumsum(onehot, axis=0) - onehot) * onehot, axis=1)
    target = chosen * capacity + slot_index
    source = jnp.repeat(jnp.arange(tokens, dtype=jnp.int32), choices_per)
    column_start = lax.axis_index("tp") * slice_width
    narrow = lax.dynamic_slice_in_dim(scaled, column_start, slice_width, 1).astype(jnp.bfloat16)
    outgoing = (
        jnp.zeros((experts * capacity, slice_width), jnp.bfloat16).at[target].set(narrow[source])
    )
    arrived = lax.all_to_all(
        outgoing.reshape(experts, capacity, slice_width),
        "ep",
        split_axis=0,
        concat_axis=0,
        tiled=True,
    )
    portion = lax.all_gather(arrived, "tp", axis=2, tiled=True)
    flat_rows = portion.reshape(experts * capacity, portion.shape[2])
    gate_rows = gate_weight[0]
    up_rows = up_weight[0]
    gate_act = jnp.dot(flat_rows, gate_rows, preferred_element_type=jnp.float32)
    up_act = jnp.dot(flat_rows, up_rows, preferred_element_type=jnp.float32)
    hidden = (jax.nn.silu(gate_act) * up_act).astype(jnp.bfloat16)
    piece_sum = jnp.dot(hidden, down_weight[0], preferred_element_type=jnp.float32).astype(
        jnp.bfloat16
    )
    summed = (
        lax.psum_scatter(piece_sum, "tp", scatter_dimension=1, tiled=True)
        .astype(jnp.float32)
        .astype(jnp.bfloat16)
    )
    returned = lax.all_to_all(
        summed.reshape(experts, capacity, slice_width),
        "ep",
        split_axis=0,
        concat_axis=0,
        tiled=True,
    )
    returned = returned.reshape(experts * capacity, slice_width)
    copies = returned[target].astype(jnp.float32).reshape(tokens, choices_per, slice_width)
    expert_out = jnp.sum(copies * route_weight[..., None], axis=1).astype(jnp.bfloat16)
    return (mixer_out, expert_out)


def solution(mesh):
    placed = (
        P(("grp", "ep"), "tp"),
        P(("grp", "ep"), "tp"),
        P(("grp", "ep"), "tp"),
        P(("grp", "ep"), "tp"),
        P(("grp", "ep"), "tp"),
        P("tp"),
        P(None, "tp"),
        P(("grp", "ep"), None),
        P(),
        P(("grp", "ep"), None),
        P(("grp", "ep"), None),
        P("ep", None, "tp"),
        P("ep", None, "tp"),
        P("ep", "tp", None),
    )
    return jax.shard_map(
        on_device,
        mesh=mesh,
        in_specs=placed,
        out_specs=(P(("grp", "ep"), "tp"), P(("grp", "ep"), "tp")),
        check_vma=False,
    )
```

profile of v0, /device:TPU:25, one launch (start us, length us, event | category | flops | bytes accessed | tf_op | source)
XLA Modules:
  0.0 277.4 jit_solution(104522305961320388)
XLA Ops:
  13.4 3.4 %scatter_custom_fusion = bf16[320,512]{1,0:T(8,128)(2,1)} fusion(s32[256]{0:T(256)S(1)} %bitcast.247, bf16[128,512]{1,0:T(8,128)(2,1)S(1)} %fusion.59, s32[1024]{0:T(1024)S(1)} %pad_clamp_fusion.1, bf16[]{:T(256)} %constant.37.clone.1), kind=kCustom, calls=%fused_computation.82 | custom fusion | bytes 327682 | tf_op jit(solution)/shard_map/scatter | solution.py:164
  16.8 4.5 %all-to-all-start = ((bf16[4,80,512]{2,1,0:T(8,128)(2,1)}), bf16[4,80,512]{2,1,0:T(8,128)(2,1)}, u32[]{:S(2)}, u32[]{:S(2)}) async-start(bf16[4,80,512]{2,1,0:T(8,128)(2,1)} %bitcast.30), calls=%async_computation | async-start | bytes 655360 | tf_op jit(solution)/shard_map/all_to_all | solution.py:166
  58.4 5.1 %pad.122 = f32[4,4,64,64]{3,2,1,0:T(8,128)} pad(f32[4,2,64,64]{3,2,1,0:T(8,128)} %pad_maximum_fusion.2, f32[]{:T(128)} %constant.24.clone.1), padding=0_0_0x0_1_1x0_0_0x0_0_0 | pad | bytes 393220 | tf_op jit(solution)/shard_map/pad | solution.py:64
  63.5 5.1 %pad.123 = f32[4,4,64,64]{3,2,1,0:T(8,128)} pad(f32[4,2,64,64]{3,2,1,0:T(8,128)} %pad_add_fusion, f32[]{:T(128)} %constant.24.clone.1), padding=0_0_0x1_0_1x0_0_0x0_0_0 | pad | bytes 393220 | tf_op jit(solution)/shard_map/pad | solution.py:64
  74.5 9.1 %pad.125 = f32[4,8,64,64]{3,2,1,0:T(8,128)} pad(f32[4,4,64,64]{3,2,1,0:T(8,128)} %add.412, f32[]{:T(128)} %constant.24.clone.1), padding=0_0_0x1_0_1x0_0_0x0_0_0 | pad | bytes 786436 | tf_op jit(solution)/shard_map/pad | solution.py:64
  85.5 9.2 %pad.124 = f32[4,8,64,64]{3,2,1,0:T(8,128)} pad(f32[4,4,64,64]{3,2,1,0:T(8,128)} %pad_maximum_fusion.1, f32[]{:T(128)} %constant.24.clone.1), padding=0_0_0x0_1_1x0_0_0x0_0_0 | pad | bytes 786436 | tf_op jit(solution)/shard_map/pad | solution.py:64
  94.7 2.9 %add.414 = f32[4,8,64,64]{3,2,1,0:T(8,128)} add(f32[4,8,64,64]{3,2,1,0:T(8,128)} %pad.124, f32[4,8,64,64]{3,2,1,0:T(8,128)} %pad.125) | non-fusion elementwise | flops 131072 | bytes 1572864 | tf_op jit(solution)/shard_map/add | solution.py:64
  101.4 6.4 %all-reduce.38 = (f32[16]{0:T(128)S(1)}, f32[16]{0:T(128)S(1)}) all-reduce(f32[16]{0:T(128)S(1)} %dynamic-update-slice, f32[16]{0:T(128)S(1)} %dynamic-update-slice.1), channel_id=2, replica_groups=mesh['grp'=2,'ep'=4,'tp'=4] {'ep'}, use_global_device_ids=true, to_apply=%add.36 | all-reduce | flops 32 | bytes 256
  109.2 11.2 %pad.127 = f32[4,16,64,64]{3,2,1,0:T(8,128)} pad(f32[4,8,64,64]{3,2,1,0:T(8,128)S(1)} %copy-done.3, f32[]{:T(128)} %constant.24.clone.1), padding=0_0_0x1_0_1x0_0_0x0_0_0 | pad | bytes 1572868 | tf_op jit(solution)/shard_map/pad | solution.py:64
  120.3 11.1 %pad.126 = f32[4,16,64,64]{3,2,1,0:T(8,128)} pad(f32[4,8,64,64]{3,2,1,0:T(8,128)S(1)} %pad_maximum_fusion, f32[]{:T(128)} %constant.24.clone.1), padding=0_0_0x0_1_1x0_0_0x0_0_0 | pad | bytes 1572868 | tf_op jit(solution)/shard_map/pad | solution.py:64
  132.4 13.1 %all-gather.2 = f32[16,1,64,64]{3,2,1,0:T(8,128)S(1)} all-gather(f32[4,1,64,64]{3,2,1,0:T(8,128)S(1)} %slice_add_fusion), channel_id=4, replica_groups=mesh['grp'=2,'ep'=4,'tp'=4] {'ep'}, dimensions={0}, use_global_device_ids=true | all-gather | bytes 327680 | tf_op jit(solution)/shard_map/all_gather | solution.py:16
  146.4 9.3 %all-gather.3 = f32[16,1,64]{2,1,0:T(1,128)S(1)} all-gather(f32[4,1,64]{2,1,0:T(1,128)S(1)} %bitcast.246), channel_id=5, replica_groups=mesh['grp'=2,'ep'=4,'tp'=4] {'ep'}, dimensions={0}, use_global_device_ids=true | all-gather | bytes 5120 | tf_op jit(solution)/shard_map/all_gather | solution.py:16
  158.7 2.5 copy.186
  166.9 5.6 %fusion.17 = (f32[4,16,128]{2,1,0:T(8,128)S(1)}, f32[4,16,128,128]{2,3,1,0:T(8,128)}) fusion(f32[4,16,128]{2,1,0:T(8,128)S(1)} %add_maximum_fusion, f32[4,16,128]{2,1,0:T(8,128)S(1)} %bitcast.235, f32[4,16,128]{2,1,0:T(8,128)S(1)} %reduce_window_sum.28, pred[128,128]{0,1:T(8,128)(4,1)S(1)} %iota_compare_fusion, bf16[4,16,128,64]{2,1,3,0:T(8,128)(2,1)S(1)} %bitcast.214, ...), kind=kOutput, calls=%fused_computation.27 | convolution fusion | flops 141549568 | bytes 6438912 | tf_op jit(solution)/shard_map/hcjd,hcsd->hcjs/dot_general | solution.py:97
  172.4 16.5 %all-gather.9.cloned.1.call-done = bf16[4,80,2048]{2,1,0:T(8,128)(2,1)} async-done(((bf16[4,80,512]{2,1,0:T(8,128)(2,1)}), bf16[4,80,2048]{2,1,0:T(8,128)(2,1)}) %all-gather.9.cloned.1.call-update) | async-done | bytes 1310736 | tf_op jit(solution)/shard_map/all_gather | solution.py:173
  188.9 4.9 %fusion.12 = f32[320,896]{1,0:T(8,128)} fusion(bf16[320,2048]{1,0:T(8,128)(2,1)} %bitcast.252, bf16[1,2048,896]{2,1,0:T(8,128)(2,1)} %param.27), kind=kOutput, calls=%fused_computation.23 | convolution fusion | flops 1174405120 | bytes 6127616 | tf_op jit(solution)/shard_map/dot_general | solution.py:177
  193.9 7.9 %fusion.14 = bf16[320,2048]{1,0:T(8,128)(2,1)} fusion(bf16[1,896,2048]{2,1,0:T(8,128)(2,1)} %param.29, bf16[320,2048]{1,0:T(8,128)(2,1)} %bitcast.253, bf16[1,2048,896]{2,1,0:T(8,128)(2,1)} %param.28, f32[320,896]{1,0:T(8,128)} %fusion.12), kind=kOutput, calls=%fused_computation.26 | convolution fusion | flops 2351185920 | bytes 11108352 | tf_op jit(solution)/shard_map/dot_general | solution.py:180
  201.9 11.2 %pad.166 = f32[4,15,64,64]{3,2,1,0:T(8,128)} pad(f32[4,8,64,64]{3,2,1,0:T(8,128)S(1)} %pad_maximum_fusion, f32[]{:T(128)} %constant.24.clone.1), padding=0_0_0x0_0_1x0_0_0x0_0_0 | pad | bytes 1507332 | tf_op jit(solution)/shard_map/slice | solution.py:84
  213.3 2.6 slice_add_fusion.10
  223.7 4.0 %reduce-scatter.2.cloned.1.call-done = bf16[320,512]{1,0:T(8,128)(2,1)} async-done(((bf16[320,2048]{1,0:T(8,128)(2,1)}), bf16[320,512]{1,0:T(8,128)(2,1)}) %reduce-scatter.2.cloned.1.call-update) | async-done | bytes 327696 | tf_op jit(solution)/shard_map/reduce_scatter | solution.py:184
  227.7 4.5 %all-to-all-start.1 = ((bf16[4,80,512]{2,1,0:T(8,128)(2,1)}), bf16[4,80,512]{2,1,0:T(8,128)(2,1)S(1)}, u32[]{:S(2)}, u32[]{:S(2)}) async-start(bf16[4,80,512]{2,1,0:T(8,128)(2,1)} %bitcast.227), calls=%async_computation.2 | async-start | bytes 655360 | tf_op jit(solution)/shard_map/all_to_all | solution.py:188
  232.4 7.5 %all-to-all-done.1 = bf16[4,80,512]{2,1,0:T(8,128)(2,1)S(1)} async-done(((bf16[4,80,512]{2,1,0:T(8,128)(2,1)}), bf16[4,80,512]{2,1,0:T(8,128)(2,1)S(1)}, u32[]{:S(2)}, u32[]{:S(2)}) %all-to-all-start.1) | async-done | bytes 327712 | tf_op jit(solution)/shard_map/all_to_all | solution.py:188
  242.7 22.2 %all-gather.7.cloned.1.call-done = bf16[2048,1024]{0,1:T(8,128)(2,1)} async-done(((bf16[2048,256]{0,1:T(8,128)(2,1)}), bf16[2048,1024]{0,1:T(8,128)(2,1)}) %all-gather.7.cloned.1.call-update) | async-done | bytes 4194320 | tf_op jit(solution)/shard_map/all_gather | solution.py:140
  264.9 5.9 %convolution_convert_fusion = bf16[2048,512]{1,0:T(8,128)(2,1)} fusion(bf16[2048,1024]{0,1:T(8,128)(2,1)} %all-gather.7.cloned.1.call-done, bf16[1024,512]{1,0:T(8,128)(2,1)S(1)} %copy-done), kind=kOutput, calls=%fused_computation.25 | convolution fusion | flops 2148532224 | bytes 7340032 | tf_op jit(solution)/shard_map/dot_general | solution.py:139
  (261 shorter events, 77.4 us)
Async XLA Ops:
  7.2 257.8 %copy-start = (bf16[1024,512]{1,0:T(8,128)(2,1)S(1)}, bf16[1024,512]{1,0:T(8,128)(2,1)}, u32[]{:S(2)}) copy-start(bf16[1024,512]{1,0:T(8,128)(2,1)} %param.22) | copy-start | bytes 3145732
  7.2 3.0 %copy-start.10 = (bf16[128,2048]{1,0:T(8,128)(2,1)S(1)}, bf16[128,2048]{1,0:T(8,128)(2,1)}, u32[]{:S(2)}) copy-start(bf16[128,2048]{1,0:T(8,128)(2,1)} %param.23) | copy-start | bytes 1572868
  7.2 14.1 %copy-start.15 = (f32[2048,4]{0,1:T(4,128)S(1)}, f32[2048,4]{0,1:T(4,128)}, u32[]{:S(2)}) copy-start(f32[2048,4]{0,1:T(4,128)} %param.20) | copy-start | bytes 98308
  8.8 13.9 %copy-start.14 = (f32[2048,4]{0,1:T(4,128)S(1)}, f32[2048,4]{0,1:T(4,128)}, u32[]{:S(2)}) copy-start(f32[2048,4]{0,1:T(4,128)} %param.19) | copy-start | bytes 98308
  12.5 13.2 %copy-start.19 = (s32[256,1]{0,1:T(1,128)}, s32[256,1]{0,1:T(1,128)S(1)}, u32[]{:S(2)}) copy-start(s32[256,1]{0,1:T(1,128)S(1)} %compare_select_fusion.2) | copy-start | bytes 3076
  16.8 144.9 %all-to-all-start = ((bf16[4,80,512]{2,1,0:T(8,128)(2,1)}), bf16[4,80,512]{2,1,0:T(8,128)(2,1)}, u32[]{:S(2)}, u32[]{:S(2)}) async-start(bf16[4,80,512]{2,1,0:T(8,128)(2,1)} %bitcast.30), calls=%async_computation | async-start | bytes 655360 | tf_op jit(solution)/shard_map/all_to_all | solution.py:166
  21.3 167.6 %all-gather.9.cloned.1.call-start = ((), (), s32[]{:S(2)}) async-start(), calls=%async_computation.4 | async-start | bytes 1638400 | tf_op jit(solution)/shard_map/all_gather | solution.py:173
  27.2 4.0 %copy-start.11 = (bf16[2048,256]{1,0:T(8,128)(2,1)S(1)}, bf16[2048,256]{1,0:T(8,128)(2,1)}, u32[]{:S(2)}) copy-start(bf16[2048,256]{1,0:T(8,128)(2,1)} %param.18) | copy-start | bytes 3145732
  63.5 10.9 %copy-start.16 = (f32[4,7]{1,0:T(4,128)S(1)}, f32[4,7]{1,0:T(4,128)}, u32[]{:S(2)}) copy-start(f32[4,7]{1,0:T(4,128)} %slice.270) | copy-start | bytes 340
  70.7 13.0 %slice-start = ((f32[4,8,64,64]{3,2,1,0:T(8,128)}), f32[4,1,64,64]{3,2,1,0:T(8,128)S(1)}, s32[]{:S(2)}) async-start(f32[4,8,64,64]{3,2,1,0:T(8,128)} %multiply_add_fusion), calls=%async_computation.6 | async-start | bytes 262144 | tf_op jit(solution)/shard_map/slice | solution.py:64
  94.7 2.9 %copy-start.1 = (f32[4,8,64,64]{3,2,1,0:T(8,128)S(1)}, f32[4,8,64,64]{3,2,1,0:T(8,128)}, u32[]{:S(2)}) copy-start(f32[4,8,64,64]{3,2,1,0:T(8,128)} %pad.125) | copy-start | bytes 1572868
  94.7 2.9 %copy-start.2 = (f32[4,8,64,64]{3,2,1,0:T(8,128)S(1)}, f32[4,8,64,64]{3,2,1,0:T(8,128)}, u32[]{:S(2)}) copy-start(f32[4,8,64,64]{3,2,1,0:T(8,128)} %pad.124) | copy-start | bytes 1572868
  97.6 10.3 %copy-start.12 = (f32[4,1,64,64]{3,2,1,0:T(8,128)S(1)}, f32[4,1,64,64]{3,2,1,0:T(8,128)}, u32[]{:S(2)}) copy-start(f32[4,1,64,64]{3,2,1,0:T(8,128)} %slice.337) | copy-start | bytes 196612
  98.7 10.5 %copy-start.3 = (f32[4,8,64,64]{3,2,1,0:T(8,128)S(1)}, f32[4,8,64,64]{3,2,1,0:T(8,128)}, u32[]{:S(2)}) copy-start(f32[4,8,64,64]{3,2,1,0:T(8,128)} %add.414) | copy-start | bytes 1572868
  120.3 25.2 %copy-start.13 = (f32[4,7,64]{1,2,0:T(8,128)S(1)}, f32[4,7,64]{1,2,0:T(8,128)}, u32[]{:S(2)}) copy-start(f32[4,7,64]{1,2,0:T(8,128)} %slice.325) | copy-start | bytes 21508
  120.3 25.4 %copy-start.17 = (f32[4,1,64]{2,0,1:T(4,128)S(1)}, f32[4,1,64]{2,0,1:T(4,128)}, u32[]{:S(2)}) copy-start(f32[4,1,64]{2,0,1:T(4,128)} %get-tuple-element.117) | copy-start | bytes 3076
  120.3 25.4 %copy-start.18 = (f32[4,1,64]{2,0,1:T(4,128)S(1)}, f32[4,1,64]{2,0,1:T(4,128)}, u32[]{:S(2)}) copy-start(f32[4,1,64]{2,0,1:T(4,128)} %get-tuple-element.118) | copy-start | bytes 3076
  158.7 8.1 %copy-start.5 = (bf16[32,8,16,128]{3,2,1,0:T(8,128)(2,1)S(1)}, bf16[32,8,16,128]{3,2,1,0:T(8,128)(2,1)}, u32[]{:S(2)}) copy-start(bf16[32,8,16,128]{3,2,1,0:T(8,128)(2,1)} %copy-done.4) | copy-start | bytes 3145732
  161.7 66.1 %reduce-scatter.2.cloned.1.call-start = ((), (), s32[]{:S(2)}) async-start(), calls=%async_computation.5 | async-start | bytes 1638400 | tf_op jit(solution)/shard_map/reduce_scatter | solution.py:184
  201.7 11.4 %copy-start.22 = (f32[256]{0:T(256)S(1)}, f32[256]{0:T(256)}, u32[]{:S(2)}) copy-start(f32[256]{0:T(256)} %param.21) | copy-start | bytes 3076
  201.7 63.2 %all-gather.7.cloned.1.call-start = ((), (), s32[]{:S(2)}) async-start(), calls=%async_computation.3 | async-start | bytes 5242880 | tf_op jit(solution)/shard_map/all_gather | solution.py:140
  222.5 9.8 %copy-start.21 = (f32[128,2]{0,1:T(2,128)S(1)}, f32[128,2]{0,1:T(2,128)}, u32[]{:S(2)}) copy-start(f32[128,2]{0,1:T(2,128)} %param.26) | copy-start | bytes 3076
  222.5 9.9 %copy-start.20 = (s32[256,1]{0,1:T(1,128)S(1)}, s32[256,1]{0,1:T(1,128)}, u32[]{:S(2)}) copy-start(s32[256,1]{0,1:T(1,128)} %copy-done.19) | copy-start | bytes 3076
  227.7 12.1 %all-to-all-start.1 = ((bf16[4,80,512]{2,1,0:T(8,128)(2,1)}), bf16[4,80,512]{2,1,0:T(8,128)(2,1)S(1)}, u32[]{:S(2)}, u32[]{:S(2)}) async-start(bf16[4,80,512]{2,1,0:T(8,128)(2,1)} %bitcast.227), calls=%async_computation.2 | async-start | bytes 655360 | tf_op jit(solution)/shard_map/all_to_all | solution.py:188
  (7 other events, 13.5 us)
Sparse Core Ops, SparseCore 0:
  161.8 27.0 all-gather.8
  201.9 25.8 reduce-scatter.1
  229.9 35.0 all-gather.6
where the time goes:
time: 282 us; the launch traced here: 277 us
  local copies, waits for them, and re-layouts  96.1 us (34%)
  waiting for transfers between devices  50.2 us (18%)
  other arithmetic  46.2 us (16%)
  matrix products  31.7 us (11%)
  blocking collectives  28.8 us (10%)
  between operations  15 us (5%)
  starting transfers between devices  9.33 us (3%)
    pad x24, local copies, waits for them, and re-layouts, memory_cells(): lax.associative_scan(combine_states, (block_end, matrix_terms, normer_ter...  52.2 us
    all_gather x2, blocking collectives, prefix(): gathered = jax.tree.map(lambda a: lax.all_gather(a, axis), part)  22.4 us
    all_gather x1, waiting for transfers between devices, on_device(): lax.all_gather(normed, 'tp', axis=1, tiled=True)  22.2 us
    all_gather x1, waiting for transfers between devices, on_device(): portion = lax.all_gather(arrived, 'tp', axis=2, tiled=True)  16.5 us
    unnamed x70, local copies, waits for them, and re-layouts  14.4 us
    slice x2, local copies, waits for them, and re-layouts, memory_cells(): member[:, :-1]  11.3 us
    add x17, other arithmetic, memory_cells(): lax.associative_scan(combine_states, (block_end, matrix_terms, normer_ter...  10 us
    add x10, other arithmetic, combine_states(): scale_early[..., None, None] * matrix_early  9.79 us
  transfers between devices with their start and end apart: 5, of which 4 were waited for; matrix products, arithmetic and copies ran while one was open for 52% of the time, Pallas kernels for 0%

commit v1 on v0

--- a/solution.py
+++ b/solution.py
@@ -1,6 +1,8 @@
 import jax
 import jax.numpy as jnp
 from jax import lax
+from jax.experimental import pallas as pl
+from jax.experimental.pallas import tpu as pltpu
 from jax.sharding import PartitionSpec as P
 
 HEAD = 64
@@ -117,6 +119,483 @@
     normed = cells * lax.rsqrt(jnp.mean(cells * cells, axis=-1, keepdims=True) + 1e-06)
     normed = (normed * head_gain.reshape(heads, 1, 1, HEAD)).astype(jnp.bfloat16)
     return normed.transpose(1, 2, 0, 3).reshape(segment_len, heads * HEAD)
+
+
+def mm(a, b, ca, cb, precision=None):
+    return lax.dot_general(
+        a, b, (((ca,), (cb,)), ((), ())), preferred_element_type=jnp.float32, precision=precision
+    )
+
+
+def iota(shape, axis):
+    return lax.broadcasted_iota(jnp.int32, shape, axis)
+
+
+def split_parts(x, count):
+    parts = []
+    for _ in range(count):
+        part = x.astype(jnp.bfloat16)
+        parts.append(part.astype(jnp.float32))
+        x = x - part.astype(jnp.float32)
+    return jnp.concatenate(parts, axis=0).astype(jnp.bfloat16)
+
+
+def lane_heads(rows, width):
+    own = iota((rows, width), 1) // HEAD == iota((rows, width), 0) % 8
+    return jnp.where(own, 1.0, 0.0)
+
+
+def spread_columns(rows8, count, width):
+    return mm(split_parts(rows8, count), lane_heads(8 * count, width).astype(jnp.bfloat16), 0, 0)
+
+
+def spread_lanes(rows8, width):
+    wide = jnp.concatenate([rows8] * (width // rows8.shape[1]), axis=1)
+    return jnp.sum(wide * lane_heads(8, width), axis=0, keepdims=True)
+
+
+def diagonal(width):
+    shape = (2 * HEAD, width)
+    return iota(shape, 0) // HEAD == (iota(shape, 1) % (2 * HEAD)) // HEAD
+
+
+def with_ones(v):
+    return jnp.concatenate([v, jnp.ones_like(v)], axis=1)
+
+
+def gate_prepare(fg, ig, decay_ref, g_ref):
+    logf = jnp.minimum(fg, 0.0) - jnp.log1p(jnp.exp(-jnp.abs(fg)))
+    upper = jnp.where(iota((BLK, BLK), 0) <= iota((BLK, BLK), 1), 1.0, 0.0)
+    decay = mm(logf, upper, 1, 0, EXACT_PRECISION)
+    g = ig - decay
+    blocks = fg.shape[0] // 8
+    decay_ref[...] = decay.reshape(blocks, 8, BLK)
+    g_ref[...] = g.reshape(blocks, 8, BLK)
+    return decay, g
+
+
+def device_state(k_ref, v_ref, fg, ig, decay_ref, g_ref, kw_ref, acc_ref):
+    decay, g = gate_prepare(fg, ig, decay_ref, g_ref)
+    rows = fg.shape[0]
+    blocks = rows // 8
+    width = k_ref.shape[1]
+    ends = jnp.broadcast_to(decay[:, BLK - 1 : BLK], (rows, BLK))
+    here, there = iota((rows, rows), 0), iota((rows, rows), 1)
+    earlier = (here % 8 == there % 8) & (there // 8 < here // 8)
+    before = mm(jnp.where(earlier, 1.0, 0.0), ends, 1, 0, EXACT_PRECISION)
+    total = (before + ends)[rows - 8 :]
+    shifted = (g - before).reshape(blocks, 8, BLK)
+    highest = jnp.max(jnp.max(shifted, axis=0), axis=-1, keepdims=True)
+    highest = jnp.broadcast_to(highest, (8, BLK))
+    kw_ref[...] = jnp.exp(shifted - highest[None])
+    acc_ref[...] = jnp.zeros_like(acc_ref)
+
+    def one(b, carry):
+        at = pl.ds(pl.multiple_of(b * BLK, BLK), BLK)
+        keys = spread_columns(kw_ref[b], 2, width) * k_ref[at, :].astype(jnp.float32)
+        keys = keys.astype(jnp.bfloat16)
+        for p in range(width // (2 * HEAD)):
+            cols = slice(2 * HEAD * p, 2 * HEAD * (p + 1))
+            acc_ref[p] += mm(keys[:, cols], with_ones(v_ref[at, cols]), 0, 0)
+        return carry
+
+    lax.fori_loop(0, blocks, one, 0, unroll=2)
+    return total, total + highest
+
+
+def folded(state):
+    state = jnp.where(diagonal(state.shape[1]), state, 0.0)
+    return state[:HEAD] + state[HEAD:]
+
+
+def unfolded(half):
+    both = jnp.concatenate([half, half], axis=0)
+    return jnp.where(diagonal(half.shape[1]), both, 0.0)
+
+
+def cell_block(b, q_ref, k_ref, v_ref, decay_ref, g_ref, gain, state_ref, m_ref):
+    at = pl.ds(pl.multiple_of(b * BLK, BLK), BLK)
+    width = q_ref.shape[1]
+    pair = 2 * HEAD
+    g, decay, m = g_ref[b], decay_ref[b], m_ref[...]
+    causal = iota((BLK, BLK), 0) >= iota((BLK, BLK), 1)
+    low = iota((BLK, pair), 1) < HEAD
+    decay_wide = spread_columns(decay, 3, width)
+    peak = jnp.maximum(m, jnp.broadcast_to(jnp.max(g, axis=-1, keepdims=True), g.shape))
+    keys_scale = spread_columns(jnp.exp(g - peak), 2, width)
+    m_wide = spread_lanes(m, width)
+    keep = spread_lanes(jnp.exp(m - peak), width)
+    m_ref[...] = peak + jnp.broadcast_to(decay[:, BLK - 1 : BLK], g.shape)
+    mean = jnp.where(diagonal(pair), 1.0 / HEAD, 0.0).astype(jnp.bfloat16)
+    out = []
+    for p in range(width // pair):
+        cols = slice(pair * p, pair * (p + 1))
+        kp = k_ref[at, cols]
+        vp = with_ones(v_ref[at, cols])
+        qf = q_ref[at, cols].astype(jnp.float32) * HEAD ** (-0.5)
+        tops, sums = [], []
+        for i in range(2):
+            h = 2 * p + i
+            qm = jnp.where(low if i == 0 else ~low, qf, 0.0).astype(jnp.bfloat16)
+            scores = mm(qm, kp, 1, 1)
+            gm = jnp.where(causal, g[h : h + 1, :], VERY_NEGATIVE)
+            top = jnp.maximum(jnp.max(gm, axis=-1, keepdims=True), m[h : h + 1, 0:1])
+            weighted = jnp.exp(gm - top) * scores
+            tops.append(top)
+            sums.append(mm(weighted.astype(jnp.bfloat16), vp, 1, 0))
+        top = jnp.where(low, tops[0], tops[1])
+        carried_scale = jnp.exp(m_wide[:, cols] - top)
+        state = state_ref[p]
+        carried = mm((qf * carried_scale).astype(jnp.bfloat16), state.astype(jnp.bfloat16), 1, 0)
+        num = jnp.where(low, sums[0][:, :pair], sums[1][:, :pair]) + carried[:, :pair]
+        den = jnp.where(low, sums[0][:, pair:], sums[1][:, pair:]) + carried[:, pair:]
+        floor = jnp.exp(-(decay_wide[:, cols] + top))
+        cells = num / jnp.maximum(jnp.abs(den), floor)
+        square = mm((cells * cells).astype(jnp.bfloat16), mean, 1, 0)
+        normed = cells * lax.rsqrt(square + 1e-06) * gain[:, cols]
+        out.append(normed.astype(jnp.bfloat16))
+        keys = (keys_scale[:, cols] * kp.astype(jnp.float32)).astype(jnp.bfloat16)
+        fresh = jnp.where(diagonal(2 * pair), mm(keys, vp, 0, 0), 0.0)
+        kept = keep[:, cols]
+        state_ref[p] = jnp.concatenate([kept, kept], axis=1) * state + fresh
+    return jnp.concatenate(out, axis=1)
+
+
+def joined(early, late, take):
+    mats, m = early
+    late_mats, late_decay, late_m = late
+    top = jnp.maximum(late_decay + m, late_m)
+    width = 2 * HEAD * len(mats)
+    old = spread_lanes(jnp.exp(late_decay + m - top), width)
+    new = spread_lanes(jnp.exp(late_m - top), width)
+    result = []
+    for p, mat in enumerate(mats):
+        cols = slice(2 * HEAD * p, 2 * HEAD * (p + 1))
+        s0 = jnp.concatenate([old[:, cols]] * 2, axis=1)
+        s1 = jnp.concatenate([new[:, cols]] * 2, axis=1)
+        result.append(jnp.where(take, s0 * mat + s1 * late_mats[p].astype(jnp.float32), mat))
+    return result, jnp.where(take, top, m)
+
+
+def gates_by_block(gates):
+    length, heads = gates.shape
+    rows = jnp.pad(gates, ((0, 0), (0, 8 - heads))).reshape(length // BLK, BLK, 8)
+    return rows.transpose(0, 2, 1).reshape(length // BLK * 8, BLK)
+
+
+MESH = pl.DeviceIdType.MESH
+
+
+def layer_kernel(
+    q_ref, k_ref, v_ref, fg_ref, ig_ref, gain_ref, x_ref, xgain_ref, routes_ref, across_ref, share_ref,
+    gate_ref, up_ref, down_ref, project_ref, mixer_ref, expert_ref,
+    decay, g, kw, acc, m, every_mats, every_marks, outgoing, flat, gate_up, down, project, hidden,
+    piece, near, far_out, far_in, copied, returned, normed,
+    load_sem, dispatch_sem, join_sem, mats_sem, marks_sem, near_sem, far_sem, return_sem, cross_sem, side_sem, pass_sem,
+):
+    ep, place = lax.axis_size("ep"), lax.axis_index("ep")
+    tp = lax.axis_index("tp")
+    core, chip = lax.rem(tp, 2), lax.div(tp, 2)
+    sibling, opposite = chip * 2 + (1 - core), (1 - chip) * 2 + core
+    tokens, choices = routes_ref.shape
+    capacity, half = outgoing.shape[1:]
+    pairs = acc.shape[0]
+    piece_width = piece.shape[2]
+    tile = gate_up.shape[2] // 2
+    tiles = gate_up.shape[0]
+
+    def remote(src, dst, sems, index, device):
+        return pltpu.make_async_remote_copy(
+            src_ref=src, dst_ref=dst, send_sem=sems.at[0, index], recv_sem=sems.at[1, index],
+            device_id=device, device_id_type=MESH,
+        )
+
+    def tile_load(source, n, side):
+        return pltpu.make_async_copy(
+            source.at[:, pl.ds(pl.multiple_of(n * tile, tile), tile)],
+            gate_up.at[n, :, pl.ds(side * tile, tile)],
+            load_sem.at[side, n],
+        )
+
+    down_load = pltpu.make_async_copy(down_ref, down, load_sem.at[0, tiles])
+    project_load = pltpu.make_async_copy(project_ref, project, load_sem.at[1, tiles])
+
+    barrier = pltpu.get_barrier_semaphore()
+    partners = [{"ep": lax.rem(place + d, ep)} for d in range(1, ep)] + [{"tp": sibling}, {"tp": opposite}]
+    for partner in partners:
+        pl.semaphore_signal(barrier, inc=1, device_id=partner, device_id_type=MESH)
+
+    def start_tile(n, carry):
+        tile_load(gate_ref, n, 0).start()
+        tile_load(up_ref, n, 1).start()
+        return carry
+
+    lax.fori_loop(0, tiles, start_tile, 0)
+    down_load.start()
+    project_load.start()
+
+    wide = x_ref[...].astype(jnp.float32)
+    inverse = lax.rsqrt(jnp.mean(wide * wide, axis=-1, keepdims=True) + 1e-06)
+    mine = pl.ds(pl.multiple_of(core * half, half), half)
+    narrow = (x_ref[:, mine].astype(jnp.float32) * inverse * xgain_ref[:, mine]).astype(jnp.bfloat16)
+    order = iota((tokens, tokens), 0) < iota((tokens, tokens), 1)
+    order = jnp.where(order, 1.0, 0.0).astype(jnp.bfloat16)
+
+    def rows_for(expert):
+        named = jnp.zeros((8, tokens), jnp.float32)
+        for k in range(choices):
+            named += jnp.where(across_ref[k : k + 1, :] == expert, 1.0, 0.0)
+        slot = mm(named.astype(jnp.bfloat16), order, 1, 0)
+        chosen = (slot[0:1] == iota((capacity, tokens), 0).astype(jnp.float32)) & (named[0:1] > 0.5)
+        pick = jnp.where(chosen, 1.0, 0.0).astype(jnp.bfloat16)
+        return mm(pick, narrow, 1, 0).astype(jnp.bfloat16)
+
+    for d in range(1, ep):
+        outgoing[d - 1] = rows_for(lax.rem(place + d, ep))
+    flat[core, place] = rows_for(place)
+    pl.semaphore_wait(barrier, len(partners))
+    dispatches = [
+        remote(outgoing.at[d - 1], flat.at[core, place], dispatch_sem, d - 1, {"ep": lax.rem(place + d, ep)})
+        for d in range(1, ep)
+    ]
+    for copy in dispatches:
+        copy.start()
+
+    total, top = device_state(k_ref, v_ref, fg_ref[...], ig_ref[...], decay, g, kw, acc)
+    for p in range(pairs):
+        every_mats[place, p] = folded(acc[p]).astype(jnp.bfloat16)
+    every_marks[place] = jnp.concatenate([total, top], axis=1)
+
+    for copy in dispatches:
+        copy.wait_recv()
+    join = remote(flat.at[core], flat.at[core], join_sem, 0, {"tp": sibling})
+    join.start()
+    states = []
+    for d in range(1, ep):
+        peer = {"ep": lax.rem(place + d, ep)}
+        states.append(remote(every_mats.at[place], every_mats.at[place], mats_sem, d - 1, peer))
+        states.append(remote(every_marks.at[place], every_marks.at[place], marks_sem, d - 1, peer))
+    for copy in states:
+        copy.start()
+    join.wait_recv()
+
+    rows = ep * capacity
+
+    def hidden_tile(n, carry):
+        tile_load(gate_ref, n, 0).wait()
+        tile_load(up_ref, n, 1).wait()
+        both = mm(flat[0].reshape(rows, half), gate_up[n, :half, :], 1, 0)
+        both += mm(flat[1].reshape(rows, half), gate_up[n, half:, :], 1, 0)
+        gate_act, up_act = both[:, :tile], both[:, tile:]
+        result = gate_act / (1.0 + jnp.exp(-gate_act)) * up_act
+        hidden[:, pl.ds(pl.multiple_of(n * tile, tile), tile)] = result.astype(jnp.bfloat16)
+        return carry
+
+    lax.fori_loop(0, tiles, hidden_tile, 0)
+    down_load.wait()
+
+    def down_piece(slot, owner):
+        cols = pl.ds(pl.multiple_of(owner * piece_width, piece_width), piece_width)
+        piece[slot] = mm(hidden[...], down[:, cols], 1, 0).astype(jnp.bfloat16)
+
+    near_copies = [remote(piece.at[i], near.at[i], near_sem, i, {"tp": sibling}) for i in range(2)]
+    down_piece(0, (1 - chip) * 2 + (1 - core))
+    near_copies[0].start()
+    down_piece(1, sibling)
+    near_copies[1].start()
+    down_piece(2, opposite)
+    near_copies[0].wait_recv()
+    joint = piece[2].astype(jnp.float32) + near[0].astype(jnp.float32)
+    far_out[...] = joint.astype(jnp.bfloat16)
+    far_copy = remote(far_out, far_in, far_sem, 0, {"tp": opposite})
+    far_copy.start()
+    down_piece(3, tp)
+
+    for copy in states:
+        copy.wait_recv()
+    held = ([jnp.zeros((HEAD, 4 * HEAD), jnp.float32)] * pairs, jnp.zeros((8, BLK), jnp.float32))
+    for j in range(ep):
+        marks = every_marks[j]
+        late = ([every_mats[j, p] for p in range(pairs)], marks[:, :BLK], marks[:, BLK:])
+        held = joined(held, late, j < place)
+    for p in range(pairs):
+        acc[p] = unfolded(held[0][p])
+    m[...] = held[1]
+    gain = gain_ref[...]
+
+    groups = cross_sem.shape[1]
+    group_rows = q_ref.shape[0] // groups
+    per_group = group_rows // BLK
+    cross, side, onward = [], [], []
+    for n in range(groups):
+        span = pl.ds(n * group_rows, group_rows)
+        own, other = normed.at[tp, span, :], normed.at[opposite, span, :]
+        cross.append(remote(own, own, cross_sem, n, {"tp": opposite}))
+        side.append(remote(own, own, side_sem, n, {"tp": sibling}))
+        onward.append(remote(other, other, pass_sem, n, {"tp": sibling}))
+
+    def one(b, carry):
+        at = pl.ds(pl.multiple_of(b * BLK, BLK), BLK)
+        normed[tp, at, :] = cell_block(b, q_ref, k_ref, v_ref, decay, g, gain, acc, m)
+        return carry
+
+    returns = [
+        remote(copied.at[lax.rem(place + d, ep)], returned.at[place], return_sem, d - 1, {"ep": lax.rem(place + d, ep)})
+        for d in range(1, ep)
+    ]
+    for n in range(groups):
+        lax.fori_loop(n * per_group, (n + 1) * per_group, one, 0)
+        cross[n].start()
+        side[n].start()
+        if n == groups // 2:
+            near_copies[1].wait_recv()
+            far_copy.wait_recv()
+            summed = piece[3].astype(jnp.float32) + near[1].astype(jnp.float32) + far_in[...].astype(jnp.float32)
+            copied[...] = summed.astype(jnp.bfloat16).reshape(copied.shape)
+            returned[place] = copied[place]
+            for copy in returns:
+                copy.start()
+        if n >= groups // 2:
+            cross[n - groups // 2].wait_recv()
+            onward[n - groups // 2].start()
+
+    for copy in returns:
+        copy.wait_recv()
+    before = iota((tokens, tokens), 1) < iota((tokens, tokens), 0)
+    before = jnp.where(before, 1.0, 0.0).astype(jnp.bfloat16)
+    result = jnp.zeros((tokens, piece_width), jnp.float32)
+    for e in range(ep):
+        named = jnp.zeros((tokens, 1), jnp.float32)
+        weight = jnp.zeros((tokens, 1), jnp.float32)
+        for k in range(choices):
+            same = routes_ref[:, k : k + 1] == e
+            named += jnp.where(same, 1.0, 0.0)
+            weight += jnp.where(same, share_ref[:, k : k + 1], 0.0)
+        named = jnp.broadcast_to(named, (tokens, capacity))
+        slot = mm(before, named.astype(jnp.bfloat16), 1, 0)
+        chosen = (slot == iota((tokens, capacity), 1).astype(jnp.float32)) & (named > 0.5)
+        pick = jnp.where(chosen, weight, 0.0)
+        coarse = pick.astype(jnp.bfloat16)
+        fine = (pick - coarse.astype(jnp.float32)).astype(jnp.bfloat16)
+        result += mm(coarse, returned[e], 1, 0) + mm(fine, returned[e], 1, 0)
+    expert_ref[...] = result.astype(jnp.bfloat16)
+
+    project_load.wait()
+    sub = 2 * BLK
+    for n in range(groups):
+        if n >= groups - groups // 2:
+            cross[n].wait_recv()
+            onward[n].start()
+        side[n].wait_recv()
+        onward[n].wait_recv()
+
+        def mixed(i, carry):
+            at = pl.ds(pl.multiple_of(i * sub, sub), sub)
+            sums = None
+            for t in range(normed.shape[0]):
+                term = mm(normed[t, at, :], project[t * normed.shape[2] : (t + 1) * normed.shape[2], :], 1, 0)
+                sums = term if sums is None else sums + term
+            mixer_ref[at, :] = sums.astype(jnp.bfloat16)
+            return carry
+
+        lax.fori_loop(n * group_rows // sub, (n + 1) * group_rows // sub, mixed, 0)
+
+    for copy in dispatches + [join] + states + near_copies + [far_copy] + returns + cross + side + onward:
+        copy.wait_send()
+
+
+def whole_layer(
+    queries, key_vectors, value_vectors, input_gate, forget_gate, head_gain, out_weight, expert_input,
+    norm_gain, routes, route_weight, gate_weight, up_weight, down_weight,
+):
+    length, width = queries.shape
+    blocks, pairs = length // BLK, width // (2 * HEAD)
+    ep, tps = lax.axis_size("ep"), lax.axis_size("tp")
+    tokens, choices = routes.shape
+    features, units = gate_weight.shape[1:]
+    capacity = 5 * tokens * choices // (4 * ep)
+    capacity = -(-capacity // 16) * 16
+    half, tile, groups = features // 2, BLK, 4
+    piece_width = features // tps
+    tiles = units // tile
+    f32, bf16 = jnp.float32, jnp.bfloat16
+    rows = pltpu.VMEM((blocks, 8, BLK), f32)
+    sems = lambda n: pltpu.SemaphoreType.DMA((2, n))
+    vmem, anywhere = pl.BlockSpec(memory_space=pltpu.VMEM), pl.BlockSpec(memory_space=pl.ANY)
+    return pl.pallas_call(
+        layer_kernel,
+        out_shape=(
+            jax.ShapeDtypeStruct((length, out_weight.shape[1]), bf16),
+            jax.ShapeDtypeStruct((tokens, piece_width), bf16),
+        ),
+        in_specs=[vmem] * 11 + [anywhere] * 4,
+        out_specs=(vmem, vmem),
+        scratch_shapes=[
+            rows,
+            rows,
+            rows,
+            pltpu.VMEM((pairs, 2 * HEAD, 4 * HEAD), f32),
+            pltpu.VMEM((8, BLK), f32),
+            pltpu.VMEM((ep, pairs, HEAD, 4 * HEAD), bf16),
+            pltpu.VMEM((ep, 8, 2 * BLK), f32),
+            pltpu.VMEM((ep - 1, capacity, half), bf16),
+            pltpu.VMEM((2, ep, capacity, half), bf16),
+            pltpu.VMEM((tiles, features, 2 * tile), bf16),
+            pltpu.VMEM((units, features), bf16),
+            pltpu.VMEM(out_weight.shape, bf16),
+            pltpu.VMEM((ep * capacity, units), bf16),
+            pltpu.VMEM((4, ep * capacity, piece_width), bf16),
+            pltpu.VMEM((2, ep * capacity, piece_width), bf16),
+            pltpu.VMEM((ep * capacity, piece_width), bf16),
+            pltpu.VMEM((ep * capacity, piece_width), bf16),
+            pltpu.VMEM((ep, capacity, piece_width), bf16),
+            pltpu.VMEM((ep, capacity, piece_width), bf16),
+            pltpu.VMEM((tps, length, width), bf16),
+            sems(tiles + 1),
+            sems(ep - 1),
+            sems(1),
+            sems(ep - 1),
+            sems(ep - 1),
+            sems(2),
+            sems(1),
+            sems(ep - 1),
+            sems(groups),
+            sems(groups),
+            sems(groups),
+        ],
+        compiler_params=pltpu.CompilerParams(
+            collective_id=0, has_side_effects=True, vmem_limit_bytes=60 * 1024 * 1024
+        ),
+    )(
+        queries,
+        key_vectors,
+        value_vectors,
+        gates_by_block(forget_gate),
+        gates_by_block(input_gate),
+        head_gain.reshape(1, width),
+        expert_input,
+        norm_gain.reshape(1, features),
+        routes,
+        routes.T,
+        route_weight,
+        gate_weight[0],
+        up_weight[0],
+        down_weight[0],
+        out_weight,
+    )
+
+
+def fits_one_kernel(queries, routes, gate_weight):
+    ep, tps = lax.axis_size("ep"), lax.axis_size("tp")
+    length, width = queries.shape
+    return (
+        tps == 4
+        and ep > 1
+        and width % (2 * HEAD) == 0
+        and length % (8 * BLK) == 0
+        and routes.shape[0] % BLK == 0
+        and gate_weight.shape[2] % BLK == 0
+    )
 
 
 def on_device(
@@ -135,6 +614,23 @@
     up_weight,
     down_weight,
 ):
+    if fits_one_kernel(queries, routes, gate_weight):
+        return whole_layer(
+            queries,
+            key_vectors,
+            value_vectors,
+            input_gate,
+            forget_gate,
+            head_gain,
+            out_weight,
+            expert_input,
+            norm_gain,
+            routes,
+            route_weight,
+            gate_weight,
+            up_weight,
+            down_weight,
+        )
     normed = memory_cells(queries, key_vectors, value_vectors, input_gate, forget_gate, head_gain)
     mixer_out = jnp.dot(
         lax.all_gather(normed, "tp", axis=1, tiled=True),

time: 282 us -> 76.2 us (0.27); the launches traced: 277 us -> 75.9 us
  local copies, waits for them, and re-layouts: 96.1 us -> 8 us
  Pallas kernels: 0 us -> 67.3 us
  waiting for transfers between devices: 50.2 us -> 0 us
  other arithmetic: 46.2 us -> 0 us
  matrix products: 31.7 us -> 0 us
  blocking collectives: 28.8 us -> 0 us
  between operations: 15 us -> 0.65 us
  starting transfers between devices: 9.33 us -> 0 us
    pallas_call x0 -> x1, Pallas kernels: none -> 67.3 us  [whole_layer(): pl.pallas_call(layer_kernel, out_shape=(jax.ShapeDtypeStruct((length, out...]
    pad x24 -> x0, local copies, waits for them, and re-layouts: 52.2 us -> none  [memory_cells(): lax.associative_scan(combine_states, (block_end, matrix_terms, normer_ter...]
    all_gather x2 -> x0, waiting for transfers between devices: 38.7 us -> none  [the longest x1 22.2 us: on_device(): lax.all_gather(normed, 'tp', axis=1, tiled=True)]
    dot_general x8 -> x0, matrix products: 31.7 us -> none  [the longest x1 7.86 us: on_device(): jnp.dot(hidden, down_weight[0], preferred_element_type=jnp.float32)]
    add x41 -> x0, other arithmetic: 23.4 us -> none  [the longest x17 10 us: memory_cells(): lax.associative_scan(combine_states, (block_end, matrix_terms, normer_ter...]
    all_gather x2 -> x0, blocking collectives: 22.4 us -> none  [prefix(): gathered = jax.tree.map(lambda a: lax.all_gather(a, axis), part)]
    slice x30 -> x0, local copies, waits for them, and re-layouts: 17.6 us -> none  [the longest x2 11.3 us: memory_cells(): member[:, :-1]]
    all_to_all x2 -> x0, starting transfers between devices: 9.06 us -> none  [the longest x1 4.53 us: on_device(): lax.all_to_all(outgoing.reshape(experts, capacity, slice_width), 'ep', sp...]
  transfers between devices with their start and end apart: 5 -> 0, of which waited for: 4 -> 0; matrix products, arithmetic and copies ran while one was open for 52% -> 0% of each run, Pallas kernels for 0% -> 0%
where the time goes in v1:
time: 76.2 us; the launch traced here: 75.9 us
  Pallas kernels  67.3 us (88%)
  local copies, waits for them, and re-layouts  8 us (10%)
    pallas_call x1, Pallas kernels, whole_layer(): pl.pallas_call(layer_kernel, out_shape=(jax.ShapeDtypeStruct((length, out...  67.3 us
    unnamed x6, local copies, waits for them, and re-layouts  6.57 us

profile of v1, /device:TPU:25, one launch (start us, length us, event | category | flops | bytes accessed | tf_op | source)
XLA Modules:
  0.0 75.9 jit_solution(13653293892037453697)
XLA Ops:
  0.6 1.4 %copy.17.share_ref = f32[128,2]{1,0:T(8,128)} copy(f32[128,2]{0,1:T(2,128)} %param.24) | data formatting | bytes 2048 | tf_op args[10]
  2.0 1.4 %copy.16.routes_ref = s32[128,2]{1,0:T(8,128)} copy(s32[128,2]{0,1:T(2,128)} %param.23) | data formatting | bytes 2048 | tf_op args[9]
  3.5 1.4 %pad_bitcast_fusion = (f32[128,128]{1,0:T(8,128)}, f32[128,128]{1,0:T(8,128)}) fusion(f32[2048,4]{0,1:T(4,128)} %param.17, f32[2048,4]{0,1:T(4,128)} %param.18), kind=kLoop, calls=%fused_computation | loop fusion | bytes 196608 | tf_op jit(solution)/shard_map/reshape | solution.py:283
  4.9 67.3 %shard_map.149 = (bf16[2048,512]{1,0:T(8,128)(2,1)}, bf16[128,512]{1,0:T(8,128)(2,1)}) custom-call(bf16[2048,256]{1,0:T(8,128)(2,1)} %q_ref.1, bf16[2048,256]{1,0:T(8,128)(2,1)} %k_ref.1, bf16[2048,256]{1,0:T(8,128)(2,1)} %v_ref.1, f32[128,128]{1,0:T(8,128)} %get-tuple-element.3.fg_ref, f32[128,128]{1,0:T(8,128)} %get-tuple-element.2.ig_ref, ...), custom_call_target="tpu_custom_call" | custom-call | tf_op jit(solution)/shard_map/pallas_call | solution.py:525
  72.2 0.0 copy-start
  72.2 3.1 %copy.20 = bf16[2048,512]{1,0:T(8,128)(2,1)} copy(bf16[2048,512]{1,0:T(8,128)(2,1)} %get-tuple-element.6) | data formatting | bytes 4194304
  75.3 0.0 copy-done
  75.3 0.7 copy.21
Async XLA Ops:
  72.2 3.1 %copy-start = (bf16[128,512]{1,0:T(8,128)(2,1)S(1)}, bf16[128,512]{1,0:T(8,128)(2,1)}, u32[]{:S(2)}) copy-start(bf16[128,512]{1,0:T(8,128)(2,1)} %get-tuple-element.7) | copy-start | bytes 393220
